TPU v7x, 512 devices: a whole 4x8x8 slice. The times are simulated.
512 devices in a mesh: sp: 32 (over z, x), tp: 16 (over y, core).
Axes of the slice: x: 4, y: 8, z: 8, core: 2. Of those that a mesh axis runs over, the one named last changes fastest.
Arguments:
- pool_input: bfloat16 [8192, 1024], P('sp', 'tp'), may hold values from -6 to 6
- pool_weight: bfloat16 [16, 64, 64], P('tp'), may hold values from -0.75 to 0.75
- pool_gain: bfloat16 [1024], P('tp'), may hold values from 0.099609375 to 1.8984375
- out_weight: bfloat16 [1024, 2048], P(None, 'tp'), may hold values from -0.1875 to 0.1875
- resid: bfloat16 [8192, 2048], P('sp', 'tp'), may hold values from -90 to 90
- norm_gain: bfloat16 [2048], P('tp'), may hold values from 0.099609375 to 1.8984375
- routes: int32 [8192, 2], P('sp'), may hold values from 0 to 31, all different within a row; in each aligned block of 256 rows (0 to 255, 256 to 511, ...) at most 32 rows name the same one
- route_weight: float32 [8192, 2], P('sp'), may hold values from 0.2 to 1
- expert_gate: bfloat16 [32, 2048, 4096], P('sp', None, 'tp'), may hold values from -0.375 to 0.375
- expert_up: bfloat16 [32, 2048, 4096], P('sp', None, 'tp'), may hold values from -0.375 to 0.375
- expert_down: bfloat16 [32, 4096, 2048], P('sp', 'tp'), may hold values from -0.0234375 to 0.0234375
Outputs:
- layer_out: bfloat16 [8192, 2048], P('sp', 'tp')
Inputs may be any that keep to these rules, and one draw needn't show every extreme that they name: `routes`: the 2 experts of a position differ. In each aligned block of 256 positions no expert is named by more than 32 assignments; some block reaches that bound.
All inputs are finite; a program needn't handle non-finite values.
Results may differ from a plain program's by a relative error of at most 0.0085.
Values may be sent and summed in bfloat16 or wider, within the bound.
No kernel may reach another device: no remote copies, remote signals or barrier semaphores. Data moves between devices by JAX's collectives and lax.ppermute only.
A program may use at most 64 MiB of HBM per device.

v0:
```python
import jax
import jax.numpy as jnp
from jax import lax
from jax.sharding import PartitionSpec as P

D = 2048
GSIZE = 64
REACH = 16
TOPK = 2
GATE_LIMIT = 7.0
GATE_ALPHA = 1.702
NORM_EPS = 1e-05


def from_behind(value, axis, steps):
    count = lax.axis_size(axis)
    first, last = (max(0, -steps), min(count, count - steps))
    return lax.ppermute(value, axis, [(source, source + steps) for source in range(first, last)])


def sent_to_all(value, axis):
    peers = lax.axis_size(axis)
    return lax.all_to_all(
        jnp.broadcast_to(value[None], (peers, *value.shape)), axis, 0, 0, tiled=True
    )


def taken_together(value, axis):
    everything = sent_to_all(value, axis)
    return jnp.sum(everything, axis=0)


def clamped_unit(gate_pre, up_pre):
    gate_cut = jnp.minimum(gate_pre, GATE_LIMIT)
    up_cut = jnp.clip(up_pre, -GATE_LIMIT, GATE_LIMIT)
    return (up_cut + 1.0) * gate_cut * jax.nn.sigmoid(GATE_ALPHA * gate_cut)


def window_pool(extended, width_of, position, tok_count):
    summed = jnp.zeros((tok_count, extended.shape[1]), jnp.float32)
    for offset in range(REACH):
        first_row = REACH - 1 - offset
        shifted = extended[first_row : first_row + tok_count]
        summed = summed + jnp.where(offset < width_of[None, :], shifted, 0.0)
    counted = jnp.minimum(position[:, None] + 1, width_of[None, :]).astype(jnp.float32)
    current = extended[REACH - 1 :]
    return (summed / counted - current).astype(jnp.bfloat16)


def slot_of(route_block, expert_count, capacity):
    flattened = route_block.reshape(-1)
    onehot = (flattened[:, None] == jnp.arange(expert_count, dtype=jnp.int32)[None, :]).astype(
        jnp.int32
    )
    earlier = jnp.cumsum(onehot, axis=0) - onehot
    ranked = jnp.sum(earlier * onehot, axis=1)
    return flattened * capacity + ranked


def on_device(
    pool_input,
    pool_weight,
    pool_gain,
    out_weight,
    resid,
    norm_gain,
    routes,
    route_weight,
    expert_gate,
    expert_up,
    expert_down,
):
    tok_rows, channels = pool_input.shape
    groups = pool_weight.shape[0]
    features = out_weight.shape[1]
    experts_all = lax.axis_size("sp") * expert_gate.shape[0]
    capacity = 2 * tok_rows * TOPK // experts_all
    tail_rows = pool_input[tok_rows - (REACH - 1) :]
    before = from_behind(tail_rows, "sp", 1)
    extended = jnp.concatenate([before, pool_input], axis=0).astype(jnp.float32)
    first_group = lax.axis_index("tp") * groups
    width_of = 2 ** (1 + (first_group + jnp.arange(channels, dtype=jnp.int32) // GSIZE) % 4)
    position = lax.axis_index("sp") * tok_rows + jnp.arange(tok_rows, dtype=jnp.int32)
    pooled = window_pool(extended, width_of, position, tok_rows)
    grouped = jnp.einsum(
        "tgc,gcd->tgd",
        pooled.reshape(tok_rows, groups, GSIZE),
        pool_weight,
        preferred_element_type=jnp.float32,
    )
    mixed_out = (
        (grouped * pool_gain.astype(jnp.float32).reshape(groups, GSIZE))
        .astype(jnp.bfloat16)
        .reshape(tok_rows, channels)
    )
    projected = jnp.dot(
        lax.all_gather(mixed_out, "tp", axis=1, tiled=True),
        out_weight,
        preferred_element_type=jnp.float32,
    )
    stored = lax.optimization_barrier((resid.astype(jnp.float32) + projected).astype(jnp.bfloat16))
    stream = stored.astype(jnp.float32)
    squares = taken_together(jnp.sum(stream * stream, axis=1), "tp")
    scale_row = lax.rsqrt(squares / D + NORM_EPS)
    normed_part = (stream * scale_row[:, None] * norm_gain.astype(jnp.float32)).astype(jnp.bfloat16)
    slot_index = slot_of(routes, experts_all, capacity)
    token_ids = jnp.repeat(jnp.arange(tok_rows, dtype=jnp.int32), TOPK)
    slot_token = (
        jnp.full((experts_all * capacity,), tok_rows, jnp.int32).at[slot_index].set(token_ids)
    )
    sent_rows = jnp.take(normed_part, slot_token, axis=0, mode="fill", fill_value=0).reshape(
        experts_all, capacity, features
    )
    gathered = lax.all_gather(
        lax.all_to_all(sent_rows, "sp", split_axis=0, concat_axis=0, tiled=True),
        "tp",
        axis=2,
        tiled=True,
    )
    sources = gathered.shape[0]
    slot_count = gathered.shape[1]
    flattened = gathered.reshape(sources * slot_count, gathered.shape[2])
    gate_pre = jnp.dot(flattened, expert_gate[0], preferred_element_type=jnp.float32)
    up_pre = jnp.dot(flattened, expert_up[0], preferred_element_type=jnp.float32)
    hidden = clamped_unit(gate_pre, up_pre).astype(jnp.bfloat16)
    down_piece = expert_down[0]
    summed = lax.psum_scatter(
        lax.dot_general(
            down_piece, hidden, (((0,), (1,)), ((), ())), preferred_element_type=jnp.float32
        ).astype(jnp.bfloat16),
        "tp",
        scatter_dimension=0,
        tiled=True,
    ).astype(jnp.float32)
    result = summed.astype(jnp.bfloat16).reshape(summed.shape[0], sources, slot_count)
    returned = lax.all_to_all(result, "sp", split_axis=1, concat_axis=1, tiled=True)
    flat_back = returned.reshape(returned.shape[0], experts_all * capacity)
    picked = (
        jnp.take(flat_back, slot_index, axis=1)
        .astype(jnp.float32)
        .reshape(flat_back.shape[0], tok_rows, TOPK)
    )
    combined = jnp.sum(picked * route_weight[None, :, :], axis=2)
    return (stream + combined.T).astype(jnp.bfloat16)


def solution(mesh):
    in_specs = (
        P("sp", "tp"),
        P("tp", None, None),
        P("tp"),
        P(None, "tp"),
        P("sp", "tp"),
        P("tp"),
        P("sp", None),
        P("sp", None),
        P("sp", None, "tp"),
        P("sp", None, "tp"),
        P("sp", "tp", None),
    )
    out_specs = P("sp", "tp")
    return jax.shard_map(
        on_device, mesh=mesh, in_specs=in_specs, out_specs=out_specs, check_vma=False
    )
```

profile of v0, /device:TPU:25, one launch (start us, length us, event | category | flops | bytes accessed | tf_op | source)
XLA Modules:
  0.0 242.8 jit_solution(6143387055872761771)
XLA Ops:
  6.5 0.9 slice.58
  7.4 3.1 %collective-permute-start = (bf16[15,64]{0,1:T(8,128)(2,1)S(1)}, bf16[15,64]{0,1:T(8,128)(2,1)S(1)}, u32[]{:S(2)}, u32[]{:S(2)}) collective-permute-start(bf16[15,64]{0,1:T(8,128)(2,1)S(1)} %slice.58), channel_id=1, source_target_pairs={{0,16},{16,32},{32,48},{48,64},{64,80},{80,96},{96,112},{112,128},... | collective-permute-start | bytes 5768 | tf_op jit(solution)/shard_map/ppermute | solution.py:18
  10.8 0.8 copy.35
  11.9 0.7 broadcast_multiply_fusion
  12.6 1.2 reduce-window.6
  13.8 0.2 slice_reduce_fusion
  14.0 0.1 copy.40
  14.2 0.1 mul.320
  14.6 2.4 %scatter_custom_fusion = s32[1024]{0:T(1024)S(1)} fusion(s32[512]{0:T(512)S(1)} %bitcast.68, s32[512]{0:T(512)S(1)} %reshape.263, s32[]{:T(128)} %constant.149.clone.1), kind=kCustom, calls=%fused_computation.92 | custom fusion | bytes 4100 | tf_op jit(solution)/shard_map/scatter | solution.py:109
  17.1 0.7 convert_element_type.62
  17.8 0.8 maximum_convert_fusion
  18.6 1.3 fusion.7
  20.0 17.9 %all-gather = bf16[256,1,1024]{0,2,1:T(8,128)(2,1)S(1)} all-gather(bf16[256,1,64]{0,2,1:T(8,128)(2,1)S(1)} %fusion.7), channel_id=2, replica_groups=mesh['sp'=32,'tp'=16] {'tp'}, dimensions={2}, use_global_device_ids=true | all-gather | bytes 557056 | tf_op jit(solution)/shard_map/all_gather | solution.py:97
  37.9 1.3 fusion.4
  39.3 0.6 broadcast_in_dim.187
  39.9 6.2 %all-to-all-start = ((f32[16,1,256]{2,1,0:T(1,128)}), f32[16,1,256]{2,1,0:T(1,128)S(1)}, u32[]{:S(2)}, u32[]{:S(2)}) async-start(f32[16,1,256]{2,1,0:T(1,128)} %broadcast_in_dim.187), calls=%async_computation | async-start | bytes 32768 | tf_op jit(solution)/shard_map/all_to_all | solution.py:23
  46.3 4.4 %all-to-all-done = f32[16,1,256]{2,1,0:T(1,128)S(1)} async-done(((f32[16,1,256]{2,1,0:T(1,128)}), f32[16,1,256]{2,1,0:T(1,128)S(1)}, u32[]{:S(2)}, u32[]{:S(2)}) %all-to-all-start) | async-done | bytes 16416 | tf_op jit(solution)/shard_map/all_to_all | solution.py:23
  50.8 3.2 %gather_fusion = bf16[1024,128]{1,0:T(8,128)(2,1)S(1)} fusion(bf16[256,128]{1,0:T(8,128)(2,1)S(1)} %fusion.24, s32[1024]{0:T(1024)S(1)} %fusion.50), kind=kCustom, calls=%fused_computation | custom fusion | bytes 528384 | tf_op jit(solution)/shard_map/jit(_take)/gather | solution.py:111
  54.0 0.2 broadcast_select_fusion
  54.2 24.2 %all_to_all.16 = bf16[32,32,128]{2,1,0:T(8,128)(2,1)} all-to-all(bf16[32,32,128]{2,1,0:T(8,128)(2,1)S(1)} %broadcast_select_fusion), channel_id=1, replica_groups=mesh['sp'=32,'tp'=16] {'sp'}, dimensions={0} | all-to-all | bytes 524288 | tf_op jit(solution)/shard_map/all_to_all | solution.py:115
  78.5 45.3 %all-gather.3.cloned.1.call-done = bf16[32,32,2048]{2,1,0:T(8,128)(2,1)} async-done(((bf16[32,32,128]{2,1,0:T(8,128)(2,1)}), bf16[32,32,2048]{2,1,0:T(8,128)(2,1)}) %all-gather.3.cloned.1.call-update) | async-done | bytes 4194320 | tf_op jit(solution)/shard_map/all_gather | solution.py:114
  123.7 4.5 %convolution_minimum_fusion = f32[1024,256]{1,0:T(8,128)} fusion(bf16[1024,2048]{1,0:T(8,128)(2,1)} %bitcast.70, bf16[1,2048,256]{2,1,0:T(8,128)(2,1)S(1)} %copy-done.3), kind=kOutput, calls=%fused_computation.4 | convolution fusion | flops 1074003968 | bytes 6291456 | tf_op jit(solution)/shard_map/dot_general | solution.py:123
  128.3 8.8 %convert_bitcast_fusion = bf16[2048,1024]{0,1:T(8,128)(2,1)} fusion(f32[1024,256]{1,0:T(8,128)} %convolution_minimum_fusion, bf16[1024,2048]{1,0:T(8,128)(2,1)} %bitcast.71, bf16[1,256,2048]{2,1,0:T(8,128)(2,1)S(1)} %copy-done, bf16[1,2048,256]{2,1,0:T(8,128)(2,1)S(1)} %copy-done.4), kind=kOutput, calls=%fused_computation.3 | convolution fusion | flops 2151940096 | bytes 11534336 | tf_op jit(solution)/shard_map/dot_general | solution.py:128
  137.1 6.4 %copy.43 = bf16[2048,1024]{1,0:T(8,128)(2,1)} copy(bf16[2048,1024]{0,1:T(8,128)(2,1)} %convert_bitcast_fusion) | data formatting | bytes 8388608
  143.5 66.1 %reduce-scatter.4.cloned.1.call-done = bf16[128,1024]{1,0:T(8,128)(2,1)} async-done(((bf16[2048,1024]{1,0:T(8,128)(2,1)}), bf16[128,1024]{1,0:T(8,128)(2,1)}) %reduce-scatter.4.cloned.1.call-update) | async-done | bytes 262160
  209.6 1.8 copy.44
  211.4 9.9 %all-to-all-start.2 = ((bf16[128,32,32]{0,2,1:T(8,128)(2,1)}), bf16[128,32,32]{0,2,1:T(8,128)(2,1)S(1)}, u32[]{:S(2)}, u32[]{:S(2)}) async-start(bf16[128,32,32]{0,2,1:T(8,128)(2,1)} %bitcast.14), calls=%async_computation.2 | async-start | bytes 524288 | tf_op jit(solution)/shard_map/all_to_all | solution.py:136
  221.6 0.2 copy.39
  221.9 10.5 %all-to-all-done.2 = bf16[128,32,32]{0,2,1:T(8,128)(2,1)S(1)} async-done(((bf16[128,32,32]{0,2,1:T(8,128)(2,1)}), bf16[128,32,32]{0,2,1:T(8,128)(2,1)S(1)}, u32[]{:S(2)}, u32[]{:S(2)}) %all-to-all-start.2) | async-done | bytes 262176 | tf_op jit(solution)/shard_map/all_to_all | solution.py:136
  232.5 1.3 gather_fusion.1
  233.8 1.5 multiply_reduce_fusion
  235.3 0.7 fusion.25
  (49 shorter events, 1.7 us)
Async XLA Ops:
  6.5 121.7 %copy-start = (bf16[1,256,2048]{2,1,0:T(8,128)(2,1)S(1)}, bf16[1,256,2048]{2,1,0:T(8,128)(2,1)}, u32[]{:S(2)}) copy-start(bf16[1,256,2048]{2,1,0:T(8,128)(2,1)} %param.21) | copy-start | bytes 3145732
  6.5 39.6 %copy-start.5 = (bf16[128]{0:T(256)(128)(2,1)S(1)}, bf16[128]{0:T(256)(128)(2,1)}, u32[]{:S(2)}) copy-start(bf16[128]{0:T(256)(128)(2,1)} %param.16) | copy-start | bytes 772
  7.4 10.3 %collective-permute-start = (bf16[15,64]{0,1:T(8,128)(2,1)S(1)}, bf16[15,64]{0,1:T(8,128)(2,1)S(1)}, u32[]{:S(2)}, u32[]{:S(2)}) collective-permute-start(bf16[15,64]{0,1:T(8,128)(2,1)S(1)} %slice.58), channel_id=1, source_target_pairs={{0,16},{16,32},{32,48},{48,64},{64,80},{80,96},{96,112},{112,128},... | collective-permute-start | bytes 5768 | tf_op jit(solution)/shard_map/ppermute | solution.py:18
  11.6 112.2 %copy-start.3 = (bf16[1,2048,256]{2,1,0:T(8,128)(2,1)S(1)}, bf16[1,2048,256]{2,1,0:T(8,128)(2,1)}, u32[]{:S(2)}) copy-start(bf16[1,2048,256]{2,1,0:T(8,128)(2,1)} %param.19) | copy-start | bytes 3145732
  39.9 10.7 %all-to-all-start = ((f32[16,1,256]{2,1,0:T(1,128)}), f32[16,1,256]{2,1,0:T(1,128)S(1)}, u32[]{:S(2)}, u32[]{:S(2)}) async-start(f32[16,1,256]{2,1,0:T(1,128)} %broadcast_in_dim.187), calls=%async_computation | async-start | bytes 32768 | tf_op jit(solution)/shard_map/all_to_all | solution.py:23
  46.1 77.6 %all-gather.3.cloned.1.call-start = ((), (), s32[]{:S(2)}) async-start(), calls=%async_computation.4 | async-start | bytes 4456448 | tf_op jit(solution)/shard_map/all_gather | solution.py:114
  54.2 74.1 %copy-start.4 = (bf16[1,2048,256]{2,1,0:T(8,128)(2,1)S(1)}, bf16[1,2048,256]{2,1,0:T(8,128)(2,1)}, u32[]{:S(2)}) copy-start(bf16[1,2048,256]{2,1,0:T(8,128)(2,1)} %param.20) | copy-start | bytes 3145732
  78.4 131.2 %reduce-scatter.4.cloned.1.call-start = ((), (), s32[]{:S(2)}) async-start(), calls=%async_computation.5 | async-start | bytes 4456448
  143.5 78.0 %copy-start.1 = (s32[256,2]{0,1:T(2,128)S(1)}, s32[256,2]{0,1:T(2,128)}, u32[]{:S(2)}) copy-start(s32[256,2]{0,1:T(2,128)} %param.17) | copy-start | bytes 6148
  143.5 78.2 %copy-start.2 = (f32[256,2]{0,1:T(2,128)S(1)}, f32[256,2]{0,1:T(2,128)}, u32[]{:S(2)}) copy-start(f32[256,2]{0,1:T(2,128)} %param.18) | copy-start | bytes 6148
  211.4 21.1 %all-to-all-start.2 = ((bf16[128,32,32]{0,2,1:T(8,128)(2,1)}), bf16[128,32,32]{0,2,1:T(8,128)(2,1)S(1)}, u32[]{:S(2)}, u32[]{:S(2)}) async-start(bf16[128,32,32]{0,2,1:T(8,128)(2,1)} %bitcast.14), calls=%async_computation.2 | async-start | bytes 524288 | tf_op jit(solution)/shard_map/all_to_all | solution.py:136
Sparse Core Ops, SparseCore 0:
  78.6 45.1 all-gather.2
  143.7 65.9 reduce-scatter.3
where the time goes:
time: 243 us
  waiting for transfers between devices  126 us (52%)
  blocking collectives  42.1 us (17%)
  starting transfers between devices  19.3 us (8%)
  local copies, waits for them, and re-layouts  19.1 us (8%)
  matrix products  16 us (7%)
  between operations  13.6 us (6%)
  other arithmetic  6.38 us (3%)
    unnamed x3, waiting for transfers between devices  66.1 us
    all_gather x1, waiting for transfers between devices, on_device(): lax.all_gather(lax.all_to_all(sent_rows, 'sp', split_axis=0, concat_axis=...  45.3 us
    all_to_all x1, blocking collectives, on_device(): lax.all_to_all(sent_rows, 'sp', split_axis=0, concat_axis=0, tiled=True)  24.2 us
    all_gather x1, blocking collectives, on_device(): lax.all_gather(mixed_out, 'tp', axis=1, tiled=True)  17.9 us
    all_to_all x1, waiting for transfers between devices, on_device(): lax.all_to_all(result, 'sp', split_axis=1, concat_axis=1, tiled=True)  10.5 us
    all_to_all x1, starting transfers between devices, on_device(): lax.all_to_all(result, 'sp', split_axis=1, concat_axis=1, tiled=True)  9.91 us
    unnamed x16, local copies, waits for them, and re-layouts  9.15 us
    dot_general x1, matrix products, on_device(): lax.dot_general(down_piece, hidden, (((0,), (1,)), ((), ())), preferred_e...  8.85 us
  transfers between devices with their start and end apart: 5, of which 4 were waited for; matrix products, arithmetic and copies ran while one was open for 3% of the time, Pallas kernels for 0%

commit v1 on v0

--- a/solution.py
+++ b/solution.py
@@ -94,7 +94,7 @@
         .reshape(tok_rows, channels)
     )
     projected = jnp.dot(
-        lax.all_gather(mixed_out, "tp", axis=1, tiled=True),
+        jnp.concatenate(lax.all_gather(mixed_out, "tp"), axis=1),
         out_weight,
         preferred_element_type=jnp.float32,
     )

time: 243 us -> 243 us (level)
    unnamed x16 -> x21, local copies, waits for them, and re-layouts: 9.15 us -> 9.24 us
where the time goes in v1:
time: 243 us; the launch traced here: 242 us
  waiting for transfers between devices  126 us (52%)
  blocking collectives  42.1 us (17%)
  local copies, waits for them, and re-layouts  19.3 us (8%)
  starting transfers between devices  19.1 us (8%)
  matrix products  15.1 us (6%)
  between operations  13.7 us (6%)
  other arithmetic  6.35 us (3%)
    unnamed x3, waiting for transfers between devices  66.1 us
    all_gather x1, waiting for transfers between devices, on_device(): lax.all_gather(lax.all_to_all(sent_rows, 'sp', split_axis=0, concat_axis=...  45.3 us
    all_to_all x1, blocking collectives, on_device(): lax.all_to_all(sent_rows, 'sp', split_axis=0, concat_axis=0, tiled=True)  24.2 us
    all_gather x1, blocking collectives, on_device(): lax.all_gather(mixed_out, 'tp')  17.9 us
    all_to_all x1, waiting for transfers between devices, on_device(): lax.all_to_all(result, 'sp', split_axis=1, concat_axis=1, tiled=True)  10.6 us
    all_to_all x1, starting transfers between devices, on_device(): lax.all_to_all(result, 'sp', split_axis=1, concat_axis=1, tiled=True)  9.72 us
    unnamed x21, local copies, waits for them, and re-layouts  9.24 us
    dot_general x1, matrix products, on_device(): lax.dot_general(down_piece, hidden, (((0,), (1,)), ((), ())), preferred_e...  8.84 us
  transfers between devices with their start and end apart: 5, of which 4 were waited for; matrix products, arithmetic and copies ran while one was open for 3% of the time, Pallas kernels for 0%

profile of v1, /device:TPU:25, one launch (start us, length us, event | category | flops | bytes accessed | tf_op | source)
XLA Modules:
  0.0 242.0 jit_solution(3326710448677380653)
XLA Ops:
  6.5 0.9 slice.58
  7.4 3.1 %collective-permute-start = (bf16[15,64]{0,1:T(8,128)(2,1)S(1)}, bf16[15,64]{0,1:T(8,128)(2,1)S(1)}, u32[]{:S(2)}, u32[]{:S(2)}) collective-permute-start(bf16[15,64]{0,1:T(8,128)(2,1)S(1)} %slice.58), channel_id=1, source_target_pairs={{0,16},{16,32},{32,48},{48,64},{64,80},{80,96},{96,112},{112,128},... | collective-permute-start | bytes 5768 | tf_op jit(solution)/shard_map/ppermute | solution.py:18
  10.8 0.8 copy.40
  11.9 0.7 broadcast_multiply_fusion
  12.6 1.2 reduce-window.6
  13.7 0.2 slice_reduce_fusion
  14.2 0.1 mul.320
  14.6 2.4 %scatter_custom_fusion = s32[1024]{0:T(1024)S(1)} fusion(s32[512]{0:T(512)S(1)} %bitcast.77, s32[512]{0:T(512)S(1)} %reshape.267, s32[]{:T(128)} %constant.149.clone.1), kind=kCustom, calls=%fused_computation.91 | custom fusion | bytes 4100 | tf_op jit(solution)/shard_map/scatter | solution.py:109
  17.1 0.7 convert_element_type.62
  17.7 0.8 maximum_convert_fusion
  18.6 1.4 fusion.7
  20.0 17.9 %all-gather = bf16[4096,1,64]{0,2,1:T(8,128)(2,1)S(1)} all-gather(bf16[256,1,64]{0,2,1:T(8,128)(2,1)S(1)} %fusion.7), channel_id=2, replica_groups=mesh['sp'=32,'tp'=16] {'tp'}, dimensions={0}, use_global_device_ids=true | all-gather | bytes 557056 | tf_op jit(solution)/shard_map/all_gather | solution.py:97
  38.0 0.2 copy.39
  38.2 0.3 fusion.4
  38.7 0.6 broadcast_in_dim.187
  39.3 6.2 %all-to-all-start = ((f32[16,1,256]{2,1,0:T(1,128)}), f32[16,1,256]{2,1,0:T(1,128)S(1)}, u32[]{:S(2)}, u32[]{:S(2)}) async-start(f32[16,1,256]{2,1,0:T(1,128)} %broadcast_in_dim.187), calls=%async_computation | async-start | bytes 32768 | tf_op jit(solution)/shard_map/all_to_all | solution.py:23
  45.7 4.4 %all-to-all-done = f32[16,1,256]{2,1,0:T(1,128)S(1)} async-done(((f32[16,1,256]{2,1,0:T(1,128)}), f32[16,1,256]{2,1,0:T(1,128)S(1)}, u32[]{:S(2)}, u32[]{:S(2)}) %all-to-all-start) | async-done | bytes 16416 | tf_op jit(solution)/shard_map/all_to_all | solution.py:23
  50.2 3.2 %gather_fusion = bf16[1024,128]{1,0:T(8,128)(2,1)S(1)} fusion(bf16[256,128]{1,0:T(8,128)(2,1)S(1)} %fusion.23, s32[1024]{0:T(1024)S(1)} %fusion.49), kind=kCustom, calls=%fused_computation | custom fusion | bytes 528384 | tf_op jit(solution)/shard_map/jit(_take)/gather | solution.py:111
  53.4 0.2 broadcast_select_fusion
  53.6 24.2 %all_to_all.16 = bf16[32,32,128]{2,1,0:T(8,128)(2,1)} all-to-all(bf16[32,32,128]{2,1,0:T(8,128)(2,1)S(1)} %broadcast_select_fusion), channel_id=1, replica_groups=mesh['sp'=32,'tp'=16] {'sp'}, dimensions={0} | all-to-all | bytes 524288 | tf_op jit(solution)/shard_map/all_to_all | solution.py:115
  77.9 45.3 %all-gather.3.cloned.1.call-done = bf16[32,32,2048]{2,1,0:T(8,128)(2,1)} async-done(((bf16[32,32,128]{2,1,0:T(8,128)(2,1)}), bf16[32,32,2048]{2,1,0:T(8,128)(2,1)}) %all-gather.3.cloned.1.call-update) | async-done | bytes 4194320 | tf_op jit(solution)/shard_map/all_gather | solution.py:114
  123.2 4.5 %convolution_minimum_fusion = f32[1024,256]{1,0:T(8,128)} fusion(bf16[1024,2048]{1,0:T(8,128)(2,1)} %bitcast.79, bf16[1,2048,256]{2,1,0:T(8,128)(2,1)S(1)} %copy-done.5), kind=kOutput, calls=%fused_computation.4 | convolution fusion | flops 1074003968 | bytes 6291456 | tf_op jit(solution)/shard_map/dot_general | solution.py:123
  127.7 8.8 %convert_bitcast_fusion = bf16[2048,1024]{0,1:T(8,128)(2,1)} fusion(f32[1024,256]{1,0:T(8,128)} %convolution_minimum_fusion, bf16[1024,2048]{1,0:T(8,128)(2,1)} %bitcast.80, bf16[1,256,2048]{2,1,0:T(8,128)(2,1)S(1)} %copy-done, bf16[1,2048,256]{2,1,0:T(8,128)(2,1)S(1)} %copy-done.6), kind=kOutput, calls=%fused_computation.3 | convolution fusion | flops 2151940096 | bytes 11534336 | tf_op jit(solution)/shard_map/dot_general | solution.py:128
  136.5 6.4 %copy.48 = bf16[2048,1024]{1,0:T(8,128)(2,1)} copy(bf16[2048,1024]{0,1:T(8,128)(2,1)} %convert_bitcast_fusion) | data formatting | bytes 8388608
  142.9 66.1 %reduce-scatter.4.cloned.1.call-done = bf16[128,1024]{1,0:T(8,128)(2,1)} async-done(((bf16[2048,1024]{1,0:T(8,128)(2,1)}), bf16[128,1024]{1,0:T(8,128)(2,1)}) %reduce-scatter.4.cloned.1.call-update) | async-done | bytes 262160
  209.0 1.8 copy.49
  210.8 9.7 %all-to-all-start.2 = ((bf16[128,32,32]{0,2,1:T(8,128)(2,1)}), bf16[128,32,32]{0,2,1:T(8,128)(2,1)S(1)}, u32[]{:S(2)}, u32[]{:S(2)}) async-start(bf16[128,32,32]{0,2,1:T(8,128)(2,1)} %bitcast.15), calls=%async_computation.2 | async-start | bytes 524288 | tf_op jit(solution)/shard_map/all_to_all | solution.py:136
  220.8 0.2 copy.44
  221.1 10.6 %all-to-all-done.2 = bf16[128,32,32]{0,2,1:T(8,128)(2,1)S(1)} async-done(((bf16[128,32,32]{0,2,1:T(8,128)(2,1)}), bf16[128,32,32]{0,2,1:T(8,128)(2,1)S(1)}, u32[]{:S(2)}, u32[]{:S(2)}) %all-to-all-start.2) | async-done | bytes 262176 | tf_op jit(solution)/shard_map/all_to_all | solution.py:136
  231.7 1.3 gather_fusion.1
  233.0 1.5 multiply_reduce_fusion
  234.5 0.6 fusion.24
  (55 shorter events, 1.9 us)
Async XLA Ops:
  6.5 121.1 %copy-start = (bf16[1,256,2048]{2,1,0:T(8,128)(2,1)S(1)}, bf16[1,256,2048]{2,1,0:T(8,128)(2,1)}, u32[]{:S(2)}) copy-start(bf16[1,256,2048]{2,1,0:T(8,128)(2,1)} %param.21) | copy-start | bytes 3145732
  6.5 31.7 %copy-start.1 = (bf16[1024,128]{1,0:T(8,128)(2,1)S(1)}, bf16[1024,128]{1,0:T(8,128)(2,1)}, u32[]{:S(2)}) copy-start(bf16[1024,128]{1,0:T(8,128)(2,1)} %param.14) | copy-start | bytes 786436
  6.5 31.7 %copy-start.2 = (bf16[256,128]{1,0:T(8,128)(2,1)S(1)}, bf16[256,128]{1,0:T(8,128)(2,1)}, u32[]{:S(2)}) copy-start(bf16[256,128]{1,0:T(8,128)(2,1)} %param.15) | copy-start | bytes 196612
  6.5 39.0 %copy-start.7 = (bf16[128]{0:T(256)(128)(2,1)S(1)}, bf16[128]{0:T(256)(128)(2,1)}, u32[]{:S(2)}) copy-start(bf16[128]{0:T(256)(128)(2,1)} %param.16) | copy-start | bytes 772
  7.4 10.3 %collective-permute-start = (bf16[15,64]{0,1:T(8,128)(2,1)S(1)}, bf16[15,64]{0,1:T(8,128)(2,1)S(1)}, u32[]{:S(2)}, u32[]{:S(2)}) collective-permute-start(bf16[15,64]{0,1:T(8,128)(2,1)S(1)} %slice.58), channel_id=1, source_target_pairs={{0,16},{16,32},{32,48},{48,64},{64,80},{80,96},{96,112},{112,128},... | collective-permute-start | bytes 5768 | tf_op jit(solution)/shard_map/ppermute | solution.py:18
  18.6 104.6 %copy-start.5 = (bf16[1,2048,256]{2,1,0:T(8,128)(2,1)S(1)}, bf16[1,2048,256]{2,1,0:T(8,128)(2,1)}, u32[]{:S(2)}) copy-start(bf16[1,2048,256]{2,1,0:T(8,128)(2,1)} %param.19) | copy-start | bytes 3145732
  39.3 10.7 %all-to-all-start = ((f32[16,1,256]{2,1,0:T(1,128)}), f32[16,1,256]{2,1,0:T(1,128)S(1)}, u32[]{:S(2)}, u32[]{:S(2)}) async-start(f32[16,1,256]{2,1,0:T(1,128)} %broadcast_in_dim.187), calls=%async_computation | async-start | bytes 32768 | tf_op jit(solution)/shard_map/all_to_all | solution.py:23
  45.5 77.7 %all-gather.3.cloned.1.call-start = ((), (), s32[]{:S(2)}) async-start(), calls=%async_computation.4 | async-start | bytes 4456448 | tf_op jit(solution)/shard_map/all_gather | solution.py:114
  53.6 74.0 %copy-start.6 = (bf16[1,2048,256]{2,1,0:T(8,128)(2,1)S(1)}, bf16[1,2048,256]{2,1,0:T(8,128)(2,1)}, u32[]{:S(2)}) copy-start(bf16[1,2048,256]{2,1,0:T(8,128)(2,1)} %param.20) | copy-start | bytes 3145732
  77.9 131.2 %reduce-scatter.4.cloned.1.call-start = ((), (), s32[]{:S(2)}) async-start(), calls=%async_computation.5 | async-start | bytes 4456448
  142.9 77.8 %copy-start.3 = (s32[256,2]{0,1:T(2,128)S(1)}, s32[256,2]{0,1:T(2,128)}, u32[]{:S(2)}) copy-start(s32[256,2]{0,1:T(2,128)} %param.17) | copy-start | bytes 6148
  142.9 78.1 %copy-start.4 = (f32[256,2]{0,1:T(2,128)S(1)}, f32[256,2]{0,1:T(2,128)}, u32[]{:S(2)}) copy-start(f32[256,2]{0,1:T(2,128)} %param.18) | copy-start | bytes 6148
  210.8 20.9 %all-to-all-start.2 = ((bf16[128,32,32]{0,2,1:T(8,128)(2,1)}), bf16[128,32,32]{0,2,1:T(8,128)(2,1)S(1)}, u32[]{:S(2)}, u32[]{:S(2)}) async-start(bf16[128,32,32]{0,2,1:T(8,128)(2,1)} %bitcast.15), calls=%async_computation.2 | async-start | bytes 524288 | tf_op jit(solution)/shard_map/all_to_all | solution.py:136
Sparse Core Ops, SparseCore 0:
  78.0 45.1 all-gather.2
  143.0 65.9 reduce-scatter.3
